TPU v7x, 1024 devices: a whole 4x8x16 slice. The times are simulated.
1024 devices in a mesh: ep: 32 (over z, core), tp: 32 (over y, x).
Axes of the slice: x: 4, y: 8, z: 16, core: 2. Of those that a mesh axis runs over, the one named last changes fastest.
Arguments:
- tokens: bfloat16 [2048, 2048], P('ep', 'tp'), as said below
- mix_gain: float32 [2048], replicated, may hold values from 0.1 to 1.9
- w_in: bfloat16 [2048, 1024], P(None, 'tp'), may hold values from -0.125 to 0.125
- a_real: float32 [64, 64], P('tp'), may hold values from -1 to -0.1
- a_imag: float32 [64, 64], P('tp'), may hold values from -3.140625 to 3.140625
- log_step: float32 [64], P('tp'), may hold values from -3 to 0
- b_coef: float32 [2, 64, 64, 16], P(None, 'tp'), may hold values from -2.5 to 2.5
- output_coefficients: float32 [2, 64, 16, 64], P(None, 'tp'), may hold values from -1.25 to 1.25
- skip: float32 [1024], P('tp'), may hold values from -6 to 6
- w_out: bfloat16 [1024, 2048], P('tp'), may hold values from -0.1875 to 0.1875
- state: float32 [2, 2048, 64, 64], P(None, 'ep', 'tp'), may hold values from -6 to 6
- ffn_gain: float32 [2048], replicated, may hold values from 0.1 to 1.9
- w_gate: bfloat16 [64, 2048, 4096], P('ep', None, 'tp'), may hold values from -0.125 to 0.125
- w_up: bfloat16 [64, 2048, 4096], P('ep', None, 'tp'), may hold values from -0.125 to 0.125
- w_down: bfloat16 [64, 4096, 2048], P('ep', 'tp'), may hold values from -0.09375 to 0.09375
- expert_ids: int32 [2048, 2], P('ep'), may hold values from 0 to 63, all different within a row; in each aligned block of 64 rows (0 to 63, 64 to 127, ...) at most 4 rows name the same one
- route_weights: float32 [2048, 2], P('ep'), may hold values from 0.3 to 1
Outputs:
- out: bfloat16 [2048, 2048], P('ep', 'tp')
- new_state: float32 [2, 2048, 64, 64], P(None, 'ep', 'tp')
Inputs may be any that keep to these rules, and one draw needn't show every extreme that they name: `expert_ids`: A token's 2 experts differ. Among the 64 rows of one index of ep no expert is named more than 4 times, a bound that some block reaches. `tokens`: feature scales differ along the model width.
All inputs are finite; a program needn't handle non-finite values.
Results may differ from a plain program's by a relative error of at most 0.007.
Values may be sent and summed in bfloat16 or wider, within the bound.
A program may use at most 32 MiB of HBM per device.

v0:
```python
import jax
import jax.numpy as jnp
from jax import lax
from jax.sharding import PartitionSpec as P

epsilon = 1e-06
highest_precision = lax.Precision.HIGHEST


def sent_to_all(x, axis):
    devices = lax.axis_size(axis)
    return lax.all_to_all(jnp.broadcast_to(x[None], (devices, *x.shape)), axis, 0, 0, tiled=True)


def laid_out(pieces, dim):
    pieces = jnp.moveaxis(pieces, 0, dim)
    dims = pieces.shape
    return pieces.reshape(*dims[:dim], dims[dim] * dims[dim + 1], *dims[dim + 2 :])


def gathered_copies(x, axis, dim):
    pieces = sent_to_all(x, axis)
    return laid_out(pieces, dim)


def cut_along(x, dim, devices):
    before, after = (x.shape[:dim], x.shape[dim + 1 :])
    return jnp.moveaxis(x.reshape(*before, devices, -1, *after), dim, 0)


def summed_on_arrival(x, axis, dim):
    devices = lax.axis_size(axis)
    pieces = lax.all_to_all(cut_along(x, dim, devices), axis, 0, 0, tiled=True)
    return jnp.sum(pieces.astype(jnp.float32), axis=0)


def sum_at_owner(x, axis, dim):
    devices = lax.axis_size(axis)
    pieces = lax.all_to_all(cut_along(x, dim, devices), axis, 0, 0, tiled=True)
    return jnp.sum(pieces, axis=0)


def over_copies(x, axis):
    everything = sent_to_all(x, axis)
    return jnp.sum(everything, axis=0)


def rms_norm(values, gain):
    scaled = values * lax.rsqrt(jnp.mean(values * values, axis=-1, keepdims=True) + epsilon)
    return scaled * gain


def state_update(drive, a_real, a_imag, log_step, b_coef, output_coefficients, skip, state):
    count = drive.shape[0]
    groups = a_real.shape[0]
    drive_float = drive.astype(jnp.float32)
    grouped = drive_float.reshape(count, groups, -1)
    step_size = jnp.exp(log_step)[:, None]
    magnitude = jnp.exp(step_size * a_real)
    decay_re = magnitude * jnp.cos(step_size * a_imag)
    decay_imaginary = magnitude * jnp.sin(step_size * a_imag)
    denominator = a_real * a_real + a_imag * a_imag
    shifted = decay_re - 1.0
    factor_re = (shifted * a_real + decay_imaginary * a_imag) / denominator
    factor_im = (decay_imaginary * a_real - shifted * a_imag) / denominator
    coef_re = factor_re[..., None] * b_coef[0] - factor_im[..., None] * b_coef[1]
    coefficient_imaginary = factor_re[..., None] * b_coef[1] + factor_im[..., None] * b_coef[0]
    push_re = jnp.einsum("gpc,sgc->sgp", coef_re, grouped, precision=highest_precision)
    push_im = jnp.einsum(
        "gpc,sgc->sgp", coefficient_imaginary, grouped, precision=highest_precision
    )
    state_real = decay_re * state[0] - decay_imaginary * state[1] + push_re
    state_imaginary = decay_re * state[1] + decay_imaginary * state[0] + push_im
    state_readout = jnp.einsum(
        "amz,daz->dam", output_coefficients[0], state_real, precision=highest_precision
    ) - jnp.einsum(
        "amz,daz->dam", output_coefficients[1], state_imaginary, precision=highest_precision
    )
    mixed = state_readout.reshape(count, -1) + skip * drive_float
    return (jax.nn.gelu(mixed).astype(jnp.bfloat16), jnp.stack([state_real, state_imaginary]))


def slot_table(expert_ids, experts, capacity):
    flat_ids = expert_ids.reshape(-1)
    onehot = (flat_ids[:, None] == jnp.arange(experts, dtype=jnp.int32)[None, :]).astype(jnp.int32)
    ranks = jnp.cumsum(onehot, axis=0) - 1
    slot_rank = jnp.sum(onehot * ranks, axis=1)
    slots = flat_ids * capacity + slot_rank
    return (slots[:, None] == jnp.arange(experts * capacity, dtype=jnp.int32)[None, :]).astype(
        jnp.float32
    )


def local(
    tokens,
    mix_gain,
    w_in,
    a_real,
    a_imag,
    log_step,
    b_coef,
    output_coefficients,
    skip,
    w_out,
    state,
    ffn_gain,
    w_gate,
    w_up,
    w_down,
    expert_ids,
    route_weights,
):
    seq_count = tokens.shape[0]
    width = tokens.shape[1]
    top_count = expert_ids.shape[1]
    ep_count = lax.axis_size("ep")
    tp_count = lax.axis_size("tp")
    model_width = width * tp_count
    local_experts = w_gate.shape[0]
    experts = local_experts * ep_count
    capacity = max(2, 2 * seq_count * top_count // experts)
    col_start = lax.axis_index("tp") * width
    whole_rows = gathered_copies(tokens, "tp", 1)
    tok_float = whole_rows.astype(jnp.float32)
    normed = rms_norm(tok_float, mix_gain).astype(jnp.bfloat16)
    drive = jnp.dot(normed, w_in, preferred_element_type=jnp.float32).astype(jnp.bfloat16)
    mixed, new_state = state_update(
        drive, a_real, a_imag, log_step, b_coef, output_coefficients, skip, state
    )
    partial_mix = jnp.dot(mixed, w_out, preferred_element_type=jnp.float32)
    placed = slot_table(expert_ids, experts, capacity)
    per_token = (
        placed.reshape(seq_count, top_count, experts * capacity).sum(axis=1).astype(jnp.bfloat16)
    )
    mix_own = sum_at_owner(partial_mix, "tp", 1)
    resid_own = (tokens.astype(jnp.float32) + mix_own).astype(jnp.bfloat16)
    resid_float = resid_own.astype(jnp.float32)
    total_squares = over_copies(jnp.sum(resid_float * resid_float, axis=1), "tp")
    gain_own = lax.dynamic_slice_in_dim(ffn_gain, col_start, width, 0)
    normed2 = (
        resid_float * lax.rsqrt(total_squares / model_width + epsilon)[:, None] * gain_own
    ).astype(jnp.bfloat16)
    send_buffer = jnp.dot(per_token.T, normed2, preferred_element_type=jnp.float32).astype(
        jnp.bfloat16
    )
    send_buffer = send_buffer.reshape(ep_count, local_experts, capacity, width)
    full_rows = gathered_copies(
        lax.all_to_all(send_buffer, "ep", split_axis=0, concat_axis=0, tiled=True), "tp", 3
    )
    gate_vals = jnp.einsum("njcd,jdf->njcf", full_rows, w_gate, preferred_element_type=jnp.float32)
    up_vals = jnp.einsum("njcd,jdf->njcf", full_rows, w_up, preferred_element_type=jnp.float32)
    hidden = (jax.nn.silu(gate_vals) * up_vals).astype(jnp.bfloat16)
    partial_out = jnp.einsum("njcf,jfd->njcd", hidden, w_down, preferred_element_type=jnp.float32)
    expert_result = summed_on_arrival(partial_out.astype(jnp.bfloat16), "tp", 3).astype(
        jnp.bfloat16
    )
    returned_rows = lax.all_to_all(expert_result, "ep", split_axis=0, concat_axis=0, tiled=True)
    returned_rows = returned_rows.reshape(experts * capacity, width).astype(jnp.float32)
    weighted = placed * route_weights.reshape(-1)[:, None]
    combined = jnp.dot(weighted, returned_rows, precision=highest_precision)
    combined = combined.reshape(seq_count, top_count, width).sum(axis=1)
    out = (resid_own.astype(jnp.float32) + combined).astype(jnp.bfloat16)
    return (out, new_state)


def solution(mesh):
    in_specs = (
        P("ep", "tp"),
        P(),
        P(None, "tp"),
        P("tp", None),
        P("tp", None),
        P("tp"),
        P(None, "tp", None, None),
        P(None, "tp", None, None),
        P("tp"),
        P("tp", None),
        P(None, "ep", "tp", None),
        P(),
        P("ep", None, "tp"),
        P("ep", None, "tp"),
        P("ep", "tp", None),
        P("ep", None),
        P("ep", None),
    )
    out_specs = (P("ep", "tp"), P(None, "ep", "tp", None))
    return jax.shard_map(local, mesh=mesh, in_specs=in_specs, out_specs=out_specs, check_vma=False)
```

profile of v0, /device:TPU:1, one launch (start us, length us, event | category | flops | bytes accessed | tf_op | source)
XLA Modules:
  0.0 216.9 jit_solution(5580352588353726208)
XLA Ops:
  0.6 0.9 broadcast_in_dim.6
  1.6 1.1 reshape.120
  2.7 10.5 %all-to-all-start = ((bf16[32,2,2048]{2,1,0:T(2,128)(2,1)}), bf16[32,2,2048]{2,1,0:T(2,128)(2,1)S(1)}, u32[]{:S(2)}, u32[]{:S(2)}) async-start(bf16[32,2,2048]{2,1,0:T(2,128)(2,1)} %reshape.120), calls=%async_computation | async-start | bytes 524288 | tf_op jit(solution)/shard_map/all_to_all | solution.py:12
  13.2 0.7 exp.10
  13.8 0.8 add_divide_fusion
  14.6 0.9 fusion.59
  15.5 8.0 %all-to-all-done = bf16[32,2,2048]{2,1,0:T(2,128)(2,1)S(1)} async-done(((bf16[32,2,2048]{2,1,0:T(2,128)(2,1)}), bf16[32,2,2048]{2,1,0:T(2,128)(2,1)S(1)}, u32[]{:S(2)}, u32[]{:S(2)}) %all-to-all-start) | async-done | bytes 262176 | tf_op jit(solution)/shard_map/all_to_all | solution.py:12
  24.4 0.6 copy.106
  28.0 1.4 reshape.122
  29.4 3.9 %all-to-all-start.1 = ((f32[32,1,4096]{2,1,0:T(1,128)}), f32[32,1,4096]{2,1,0:T(1,128)S(1)}, u32[]{:S(2)}, u32[]{:S(2)}) async-start(f32[32,1,4096]{2,1,0:T(1,128)} %reshape.122), calls=%async_computation.1 | async-start | bytes 1048576 | tf_op jit(solution)/shard_map/all_to_all | solution.py:39
  34.3 12.0 %all-to-all-done.1 = f32[32,1,4096]{2,1,0:T(1,128)S(1)} async-done(((f32[32,1,4096]{2,1,0:T(1,128)}), f32[32,1,4096]{2,1,0:T(1,128)S(1)}, u32[]{:S(2)}, u32[]{:S(2)}) %all-to-all-start.1) | async-done | bytes 524320 | tf_op jit(solution)/shard_map/all_to_all | solution.py:39
  46.8 1.9 reduce.4
  49.3 0.6 broadcast_in_dim.7
  49.9 3.8 %all-to-all-start.2 = ((f32[32,1,64]{2,1,0:T(1,128)}), f32[32,1,64]{2,1,0:T(1,128)S(1)}, u32[]{:S(2)}, u32[]{:S(2)}) async-start(f32[32,1,64]{2,1,0:T(1,128)} %broadcast_in_dim.7), calls=%async_computation.2 | async-start | bytes 32768 | tf_op jit(solution)/shard_map/all_to_all | solution.py:12
  53.9 0.8 dynamic_slice.3
  54.6 7.7 %all-to-all-done.2 = f32[32,1,64]{2,1,0:T(1,128)S(1)} async-done(((f32[32,1,64]{2,1,0:T(1,128)}), f32[32,1,64]{2,1,0:T(1,128)S(1)}, u32[]{:S(2)}, u32[]{:S(2)}) %all-to-all-start.2) | async-done | bytes 8224 | tf_op jit(solution)/shard_map/all_to_all | solution.py:12
  62.9 40.2 %all_to_all.36 = bf16[32,2,256]{2,1,0:T(2,128)(2,1)S(1)} all-to-all(bf16[32,2,256]{2,1,0:T(2,128)(2,1)S(1)} %reshape.124), channel_id=1, replica_groups=mesh['ep'=32,'tp'=32] {'ep'}, dimensions={0} | all-to-all | bytes 65536 | tf_op jit(solution)/shard_map/all_to_all | solution.py:148
  103.7 2.3 %reshape.126 = bf16[32,2,8192]{2,1,0:T(2,128)(2,1)} reshape(bf16[32,2,4,32,64]{4,3,2,1,0:T(8,128)(2,1)S(1)} %broadcast_bitcast_fusion) | data formatting | bytes 2097152
  106.0 30.6 %all_to_all.37 = bf16[32,2,8192]{2,1,0:T(2,128)(2,1)} all-to-all(bf16[32,2,8192]{2,1,0:T(2,128)(2,1)} %reshape.126), channel_id=1, replica_groups=mesh['ep'=32,'tp'=32] {'tp'}, dimensions={0} | all-to-all | bytes 2097152 | tf_op jit(solution)/shard_map/all_to_all | solution.py:12
  136.6 3.8 %reshape.127 = bf16[32,2,4,32,64]{4,3,2,1,0:T(8,128)(2,1)S(1)} reshape(bf16[32,2,8192]{2,1,0:T(2,128)(2,1)} %all_to_all.37) | data formatting | bytes 2097152
  140.8 2.7 %copy.113 = bf16[32,2,4,32,64]{4,3,0,2,1:T(8,128)(2,1)} copy(bf16[32,2,4,32,64]{4,0,2,1,3:T(8,128)(2,1)S(1)} %bitcast_bitcast_fusion) | data formatting | bytes 2097152 | tf_op jit(solution)/shard_map/transpose | solution.py:16
  143.6 3.5 %reshape.112 = bf16[32,2,4,2048]{3,0,2,1:T(8,128)(2,1)S(1)} reshape(bf16[32,2,4,32,64]{4,3,0,2,1:T(8,128)(2,1)} %copy.113) | data formatting | bytes 2097152 | tf_op jit(solution)/shard_map/reshape | solution.py:18
  147.5 2.9 %fusion = bf16[32,2,4,2048]{3,0,2,1:T(8,128)(2,1)} fusion(bf16[32,2,4,2048]{3,0,2,1:T(8,128)(2,1)S(1)} %reshape.112, bf16[2,128,2048]{2,1,0:T(8,128)(2,1)S(1)} %copy-done, bf16[2,2048,128]{2,1,0:T(8,128)(2,1)} %param.30, f32[32,2,4,128]{3,0,2,1:T(8,128)S(1)} %convolution_bitcast_fusion.1), kind=kOutput, calls=%fused_computation.1 | convolution fusion | flops 269156352 | bytes 4325376 | tf_op jit(solution)/shard_map/njcf,jfd->njcd/dot_general | solution.py:153
  150.4 3.3 %reshape.113 = bf16[32,2,4,32,64]{4,3,0,2,1:T(8,128)(2,1)S(1)} reshape(bf16[32,2,4,2048]{3,0,2,1:T(8,128)(2,1)} %fusion) | data formatting | bytes 2097152 | tf_op jit(solution)/shard_map/reshape | solution.py:28
  153.7 2.2 copy.142
  155.9 3.9 %reshape.128 = bf16[32,2,8192]{2,1,0:T(2,128)(2,1)S(1)} reshape(bf16[32,2,4,32,64]{4,3,2,1,0:T(8,128)(2,1)} %bitcast.129) | data formatting | bytes 2097152
  159.8 31.7 %all_to_all.38 = bf16[32,2,8192]{2,1,0:T(2,128)(2,1)} all-to-all(bf16[32,2,8192]{2,1,0:T(2,128)(2,1)S(1)} %reshape.128), channel_id=1, replica_groups=mesh['ep'=32,'tp'=32] {'tp'}, dimensions={0} | all-to-all | bytes 2097152 | tf_op jit(solution)/shard_map/all_to_all | solution.py:33
  191.5 3.8 %reshape.129 = bf16[32,2,4,32,64]{4,3,2,1,0:T(8,128)(2,1)S(1)} reshape(bf16[32,2,8192]{2,1,0:T(2,128)(2,1)} %all_to_all.38) | data formatting | bytes 2097152
  195.7 0.7 reshape.130
  196.4 7.2 %all-to-all-start.6 = ((bf16[32,2,256]{2,1,0:T(2,128)(2,1)}), bf16[32,2,256]{2,1,0:T(2,128)(2,1)S(1)}, u32[]{:S(2)}, u32[]{:S(2)}) async-start(bf16[32,2,256]{2,1,0:T(2,128)(2,1)} %reshape.130), calls=%async_computation.6 | async-start | bytes 65536 | tf_op jit(solution)/shard_map/all_to_all | solution.py:157
  203.7 0.8 copy.118
  204.4 11.5 %all-to-all-done.6 = bf16[32,2,256]{2,1,0:T(2,128)(2,1)S(1)} async-done(((bf16[32,2,256]{2,1,0:T(2,128)(2,1)}), bf16[32,2,256]{2,1,0:T(2,128)(2,1)S(1)}, u32[]{:S(2)}, u32[]{:S(2)}) %all-to-all-start.6) | async-done | bytes 32800 | tf_op jit(solution)/shard_map/all_to_all | solution.py:157
  (65 shorter events, 9.2 us)
Async XLA Ops:
  0.6 146.8 %copy-start = (bf16[2,128,2048]{2,1,0:T(8,128)(2,1)S(1)}, bf16[2,128,2048]{2,1,0:T(8,128)(2,1)}, u32[]{:S(2)}) copy-start(bf16[2,128,2048]{2,1,0:T(8,128)(2,1)} %param.31) | copy-start | bytes 3145732
  2.7 20.9 %all-to-all-start = ((bf16[32,2,2048]{2,1,0:T(2,128)(2,1)}), bf16[32,2,2048]{2,1,0:T(2,128)(2,1)S(1)}, u32[]{:S(2)}, u32[]{:S(2)}) async-start(bf16[32,2,2048]{2,1,0:T(2,128)(2,1)} %reshape.120), calls=%async_computation | async-start | bytes 524288 | tf_op jit(solution)/shard_map/all_to_all | solution.py:12
  24.3 1.1 copy-start.2
  24.3 1.1 copy-start.7
  24.3 1.3 copy-start.5
  24.3 1.8 copy-start.6
  24.3 2.2 %copy-start.9 = (f32[32]{0:T(128)S(1)}, f32[32]{0:T(128)}, u32[]{:S(2)}) copy-start(f32[32]{0:T(128)} %param.25) | copy-start | bytes 388
  24.4 2.3 %copy-start.3 = (bf16[32,2048]{1,0:T(8,128)(2,1)S(1)}, bf16[32,2048]{1,0:T(8,128)(2,1)}, u32[]{:S(2)}) copy-start(bf16[32,2048]{1,0:T(8,128)(2,1)} %param.26) | copy-start | bytes 393220
  27.4 6.0 %copy-start.8 = (s32[64,2]{0,1:T(2,128)S(1)}, s32[64,2]{0,1:T(2,128)}, u32[]{:S(2)}) copy-start(s32[64,2]{0,1:T(2,128)} %param.32) | copy-start | bytes 1540
  29.4 16.8 %all-to-all-start.1 = ((f32[32,1,4096]{2,1,0:T(1,128)}), f32[32,1,4096]{2,1,0:T(1,128)S(1)}, u32[]{:S(2)}, u32[]{:S(2)}) async-start(f32[32,1,4096]{2,1,0:T(1,128)} %reshape.122), calls=%async_computation.1 | async-start | bytes 1048576 | tf_op jit(solution)/shard_map/all_to_all | solution.py:39
  33.3 15.9 %copy-start.4 = (bf16[64,64]{1,0:T(8,128)(2,1)S(1)}, bf16[64,64]{1,0:T(8,128)(2,1)}, u32[]{:S(2)}) copy-start(bf16[64,64]{1,0:T(8,128)(2,1)} %param.17) | copy-start | bytes 24580
  49.9 12.4 %all-to-all-start.2 = ((f32[32,1,64]{2,1,0:T(1,128)}), f32[32,1,64]{2,1,0:T(1,128)S(1)}, u32[]{:S(2)}, u32[]{:S(2)}) async-start(f32[32,1,64]{2,1,0:T(1,128)} %broadcast_in_dim.7), calls=%async_computation.2 | async-start | bytes 32768 | tf_op jit(solution)/shard_map/all_to_all | solution.py:12
  143.6 3.5 %copy-start.1 = (bf16[2,2048,128]{2,1,0:T(8,128)(2,1)S(1)}, bf16[2,2048,128]{2,1,0:T(8,128)(2,1)}, u32[]{:S(2)}) copy-start(bf16[2,2048,128]{2,1,0:T(8,128)(2,1)} %param.29) | copy-start | bytes 3145732
  195.2 20.8 %copy-start.10 = (f32[64,2]{0,1:T(2,128)S(1)}, f32[64,2]{0,1:T(2,128)}, u32[]{:S(2)}) copy-start(f32[64,2]{0,1:T(2,128)} %param.33) | copy-start | bytes 1540
  196.4 19.5 %all-to-all-start.6 = ((bf16[32,2,256]{2,1,0:T(2,128)(2,1)}), bf16[32,2,256]{2,1,0:T(2,128)(2,1)S(1)}, u32[]{:S(2)}, u32[]{:S(2)}) async-start(bf16[32,2,256]{2,1,0:T(2,128)(2,1)} %reshape.130), calls=%async_computation.6 | async-start | bytes 65536 | tf_op jit(solution)/shard_map/all_to_all | solution.py:157
where the time goes:
time: 218 us; the launch traced here: 217 us
  blocking collectives  103 us (47%)
  waiting for transfers between devices  39.2 us (18%)
  local copies, waits for them, and re-layouts  38.4 us (18%)
  starting transfers between devices  25.4 us (12%)
  matrix products  5.27 us (2%)
  other arithmetic  4.97 us (2%)
    all_to_all x1, blocking collectives, local(): lax.all_to_all(send_buffer, 'ep', split_axis=0, concat_axis=0, tiled=True)  40.2 us
    all_to_all x1, blocking collectives, summed_on_arrival(): pieces = lax.all_to_all(cut_along(x, dim, devices), axis, 0, 0, tiled=True)  31.7 us
    all_to_all x1, blocking collectives, sent_to_all(): lax.all_to_all(jnp.broadcast_to(x[None], (devices, *x.shape)), axis, 0, 0...  30.6 us
    unnamed x37, local copies, waits for them, and re-layouts  19.5 us
    all_to_all x2, waiting for transfers between devices, sent_to_all(): lax.all_to_all(jnp.broadcast_to(x[None], (devices, *x.shape)), axis, 0, 0...  15.7 us
    all_to_all x2, starting transfers between devices, sent_to_all(): lax.all_to_all(jnp.broadcast_to(x[None], (devices, *x.shape)), axis, 0, 0...  14.3 us
    all_to_all x1, waiting for transfers between devices, sum_at_owner(): pieces = lax.all_to_all(cut_along(x, dim, devices), axis, 0, 0, tiled=True)  12 us
    all_to_all x1, waiting for transfers between devices, local(): lax.all_to_all(expert_result, 'ep', split_axis=0, concat_axis=0, tiled=True)  11.5 us
  transfers between devices with their start and end apart: 4, of which 4 were waited for; matrix products, arithmetic and copies ran while one was open for 2% of the time, Pallas kernels for 0%

commit v1 on v0

v1 whole, which is shorter than its diff:
```python
import jax
import jax.numpy as jnp
from jax import lax
from jax.experimental import pallas as pl
from jax.experimental.pallas import tpu as pltpu
from jax.sharding import PartitionSpec as P

EPS = 1e-06
HI = lax.Precision.HIGHEST
MESH = pl.DeviceIdType.MESH
NT = (((1,), (1,)), ((), ()))
TN = (((0,), (0,)), ((), ()))
F32 = jnp.float32
BF16 = jnp.bfloat16
NX, NY = 4, 8
TP, EP = 32, 32
NEAR = (0, 1, 7, 2, 6, 3, 5, 4)
FAR = (4, 3, 5, 2, 6, 1, 7, 0)


def iota(shape, dim):
    return lax.broadcasted_iota(jnp.int32, shape, dim)


def lo_lanes(rows, lanes=128):
    return iota((rows, lanes), 1) % 128 < 64


def swap(x):
    return pltpu.roll(x, 64, axis=x.ndim - 1)


def far_first(i):
    return 16 + ((i + 1) // 2) * (2 * (i % 2) - 1) * -1


def body(
    tok_ref, gain1_ref, win_hbm, ar_ref, ai_ref, ls_ref, b_ref, oc_ref, skip_ref, wout_ref,
    state_ref, gain2_ref, wg_hbm, wu_hbm, wd_hbm, ids_ref, rw_ref,
    out_ref, ns_ref,
    ta, ma, ws, wo, zs, zr, xf, yf, ro, rl, rr, ry, qs, qr, win2, wi, wdr, wd2,
    gd1, gd2, seltv, wtv, tokd,
    load_sem, sa, sw, sm, sz, sx, se, sq, ra, rw_sem, rm, rz, rq, rdy, rdl, rdr, rdo,
    reo, rel, rer, rey,
):
    t = lax.axis_index("tp")
    e = lax.axis_index("ep")
    y = t // NX
    x = t % NX
    xp = lax.rem(x + 1, NX)
    xm = lax.rem(x + NX - 1, NX)
    xo = lax.rem(x + 2, NX)

    loads = [
        pltpu.make_async_copy(win_hbm, win2.at[:, 0], load_sem.at[0]),
        pltpu.make_async_copy(win_hbm, win2.at[:, 1], load_sem.at[1]),
        pltpu.make_async_copy(wd_hbm, wdr, load_sem.at[2]),
    ]
    for j in range(2):
        loads.append(
            pltpu.make_async_copy(wg_hbm.at[j], wi.at[:, j, :, pl.ds(0, 128)], load_sem.at[3 + j])
        )
        loads.append(
            pltpu.make_async_copy(wu_hbm.at[j], wi.at[:, j, :, pl.ds(128, 128)], load_sem.at[5 + j])
        )
    barrier = pltpu.get_barrier_semaphore()

    def greet(i, c):
        d = far_first(i)
        pl.semaphore_signal(
            barrier, inc=1, device_id={"ep": lax.rem(e + d, EP)}, device_id_type=MESH
        )
        pl.semaphore_signal(
            barrier, inc=1, device_id={"tp": lax.rem(t + d, TP)}, device_id_type=MESH
        )
        return c

    lax.fori_loop(0, 31, greet, 0)
    for c in loads:
        c.start()

    tok = tok_ref[...]
    spread = (iota((64, 128), 1) % 64 == iota((64, 128), 0)).astype(F32)
    lo64 = lo_lanes(64)
    spread_lo = jnp.where(lo64, spread, 0.0).astype(BF16)
    spread_hi = jnp.where(lo64, 0.0, spread).astype(BF16)
    packed = jnp.dot(tok[0:32], spread_lo, preferred_element_type=F32) + jnp.dot(
        tok[32:64], spread_hi, preferred_element_type=F32
    )
    ta[t] = packed.astype(BF16)
    tokd[...] = jnp.dot(tok, spread.astype(BF16), preferred_element_type=F32)

    lo16 = lo_lanes(16)
    for k in range(16):
        blk = wout_ref[:, k * 128 : (k + 1) * 128].astype(F32)
        top, bot = blk[0:16], blk[16:32]
        ws[2 * k] = jnp.where(lo16, top, swap(bot)).astype(BF16)
        ws[2 * k + 1] = jnp.where(lo16, swap(top), bot).astype(BF16)
    wo[t] = ws[t]

    pl.semaphore_wait(barrier, 62)

    def to_tp(src, dst, send, recv):
        def one(i, c):
            dest = lax.rem(t + far_first(i), TP)
            pltpu.make_async_remote_copy(
                src_ref=src(dest), dst_ref=dst, send_sem=send, recv_sem=recv,
                device_id={"tp": dest}, device_id_type=MESH,
            ).start()
            return c

        lax.fori_loop(0, 31, one, 0)

    def to_ep(src, dst, send, recv):
        def one(i, c):
            dest = lax.rem(e + far_first(i), EP)
            pltpu.make_async_remote_copy(
                src_ref=src.at[dest], dst_ref=dst.at[e], send_sem=send, recv_sem=recv,
                device_id={"ep": dest}, device_id_type=MESH,
            ).start()
            return c

        lax.fori_loop(0, 31, one, 0)

    def all_of(ref, send, recv):
        r = ref.at[pl.ds(0, 31)]
        return pltpu.make_async_remote_copy(
            src_ref=r, dst_ref=r, send_sem=send, recv_sem=recv,
            device_id={"tp": lax.rem(t + 1, TP)}, device_id_type=MESH,
        )

    to_tp(lambda d: ta.at[t], ta.at[t], sa, ra)
    to_tp(lambda d: ws.at[d], wo.at[t], sw, rw_sem)

    ids = ids_ref[...]
    rw = rw_ref[...]
    lane = iota((64, 128), 1)
    id0, id1 = ids[:, 0:1], ids[:, 1:2]
    w0, w1 = rw[:, 0:1], rw[:, 1:2]
    below = (iota((64, 64), 1) < iota((64, 64), 0)).astype(F32).astype(BF16)
    sels = []
    for j in range(2):
        named = 2 * (lane // 4) + j
        hit0 = (id0 == named).astype(F32)
        hit1 = (id1 == named).astype(F32)
        hit = hit0 + hit1
        rank = jnp.dot(below, hit.astype(BF16), preferred_element_type=F32)
        here = (rank.astype(jnp.int32) == lane % 4).astype(F32)
        sels.append(hit * here)
        wtv[j] = (hit0 * w0 + hit1 * w1) * here
    seltv[...] = jnp.concatenate(sels, axis=0).T.astype(BF16)

    for src, dst in ((gain1_ref, gd1), (gain2_ref, gd2)):
        g = src[...]
        s = swap(g)
        lo = lo_lanes(16)
        dst[0] = jnp.where(lo, g, s)
        dst[1] = jnp.where(lo, s, g)

    loads[2].wait()
    lo128 = lo_lanes(128)
    for k in range(16):
        for j in range(2):
            blk = wdr[j, :, k * 128 : (k + 1) * 128].astype(F32)
            rolled = swap(blk)
            even, odd = (blk, rolled) if j == 0 else (rolled, blk)
            keep = lo128 if j == 0 else jnp.logical_not(lo128)
            for tt, piece in ((2 * k, even), (2 * k + 1, odd)):
                pos = (tt % NX) * NY + tt // NX
                wd2[pos, j * 128 : (j + 1) * 128, :] = jnp.where(keep, piece, 0.0).astype(BF16)
    for i in (0, 1, 3, 4, 5, 6):
        loads[i].wait()

    all_of(ta, sa, ra).wait_recv()
    lo32 = lo_lanes(32)
    acc = jnp.zeros((32, 128), F32)
    for k in range(TP):
        v = ta[k].astype(F32)
        acc = acc + v * v
    s0 = jnp.sum(jnp.where(lo32, acc, 0.0), axis=1, keepdims=True)
    s1 = jnp.sum(jnp.where(lo32, 0.0, acc), axis=1, keepdims=True)
    scale = jnp.where(
        lo32, lax.rsqrt(s0 / 2048.0 + EPS), lax.rsqrt(s1 / 2048.0 + EPS)
    )
    blocks = []
    for k in range(TP):
        v = ta[k].astype(F32) * scale * gd1[k % 2, k // 2 : k // 2 + 1, :]
        blocks.append(
            jnp.concatenate(
                [jnp.where(lo32, v, 0.0).astype(BF16), jnp.where(lo32, 0.0, v).astype(BF16)], axis=0
            )
        )
    drive = jnp.dot(
        jnp.concatenate(blocks, axis=1), win2[...].reshape(4096, 32), preferred_element_type=F32
    )
    drive = drive.astype(BF16).astype(F32)

    readout = skip_ref[...] * drive
    zeros16 = jnp.zeros((16, 64), F32)
    for g in range(2):
        step = jnp.exp(jnp.full((1, 64), ls_ref[g], F32))
        ar, ai = ar_ref[g : g + 1, :], ai_ref[g : g + 1, :]
        mag = jnp.exp(step * ar)
        dr, di = mag * jnp.cos(step * ai), mag * jnp.sin(step * ai)
        den = ar * ar + ai * ai
        sh = dr - 1.0
        fr, fi = (sh * ar + di * ai) / den, (di * ar - sh * ai) / den
        u = drive[:, g * 16 : (g + 1) * 16]
        q0 = lax.dot_general(u, b_ref[0, g], NT, precision=HI, preferred_element_type=F32)
        q1 = lax.dot_general(u, b_ref[1, g], NT, precision=HI, preferred_element_type=F32)
        p0, p1 = state_ref[0, :, g, :], state_ref[1, :, g, :]
        n0 = dr * p0 - di * p1 + (fr * q0 - fi * q1)
        n1 = dr * p1 + di * p0 + (fr * q1 + fi * q0)
        ns_ref[0, :, g, :] = n0
        ns_ref[1, :, g, :] = n1
        order = (lambda o: [o, zeros16]) if g == 0 else (lambda o: [zeros16, o])
        c0 = jnp.concatenate(order(oc_ref[0, g]), axis=0)
        c1 = jnp.concatenate(order(oc_ref[1, g]), axis=0)
        readout = readout + (
            lax.dot_general(n0, c0, NT, precision=HI, preferred_element_type=F32)
            - lax.dot_general(n1, c1, NT, precision=HI, preferred_element_type=F32)
        )
    mixed = jax.nn.gelu(readout)
    first = iota((64, 32), 1) < 16
    stacked = jnp.concatenate(
        [jnp.where(first, mixed, 0.0), jnp.where(first, 0.0, mixed)], axis=0
    ).astype(BF16)
    pick = (iota((16, 32), 1) % 16 == iota((16, 32), 0)).astype(F32).astype(BF16)
    ma[t] = lax.dot_general(pick, stacked, NT, preferred_element_type=F32).astype(BF16)
    to_tp(lambda d: ma.at[t], ma.at[t], sm, rm)

    all_of(wo, sw, rw_sem).wait_recv()
    all_of(ma, sm, rm).wait_recv()
    prod = lax.dot_general(
        ma[...].reshape(512, 128), wo[...].reshape(512, 128), TN, preferred_element_type=F32
    )
    half = jnp.where(lo64, prod[0:64], prod[64:128])
    resid = (tokd[...] + (half + swap(half))).astype(BF16)
    resid_f = resid.astype(F32)
    tokd[...] = resid_f

    zero = jnp.zeros((64, 128), F32)
    diag = jnp.concatenate(
        [jnp.where(lo64, resid_f, zero), jnp.where(lo64, zero, resid_f)], axis=0
    ).astype(BF16)
    sent = jnp.dot(seltv[...], diag, preferred_element_type=F32)
    ZPACK(zs, sent)
    zr[e] = zs[e]
    to_ep(zs, zr, sz, rz)
    all_of(zr, sz, rz).wait_recv()
    xf[x * NY + y] = ZUNPACK(zr)

    def push(src, dst, ssem, rsem, dy=None, dx=None):
        py = y if dy is None else lax.rem(y + dy, NY)
        px = x if dx is None else dx
        c = pltpu.make_async_remote_copy(
            src_ref=src, dst_ref=dst, send_sem=ssem, recv_sem=rsem,
            device_id={"tp": py * NX + px}, device_id_type=MESH,
        )
        c.start()

    def arrived(ref, rsem):
        pltpu.make_async_remote_copy(
            src_ref=ref, dst_ref=ref, send_sem=sx, recv_sem=rsem,
            device_id={"tp": lax.rem(t + 1, TP)}, device_id_type=MESH,
        ).wait_recv()

    mine = xf.at[x * NY + y]
    for d in (4, 3, 5, 2, 6, 1, 7):
        push(mine, mine, sx, rdy.at[d], dy=d)

    def at_y(off):
        return lax.rem(y + off, NY)

    def relay(k):
        yk = at_y(NEAR[k])
        if k % 2 == 0:
            ref = xf.at[xm * NY + yk]
            arrived(ref, rdl.at[k])
            push(ref, ref, sx, rdo.at[k], dx=xp)
        else:
            ref = xf.at[xp * NY + yk]
            arrived(ref, rdr.at[k])
            push(ref, ref, sx, rdo.at[k], dx=xm)

    for k in range(8):
        ref = xf.at[x * NY + at_y(NEAR[k])]
        if k > 0:
            arrived(ref, rdy.at[(8 - NEAR[k]) % 8])
        push(ref, ref, sx, rdl.at[k], dx=xp)
        push(ref, ref, sx, rdr.at[k], dx=xm)
        if k >= 3:
            relay(k - 3)
    for k in range(5, 8):
        relay(k)

    lo256 = lo_lanes(128, 256)

    def slab(xs, acc, ssq):
        for k in range(4):
            xa = xf[xs * NY + 2 * k].astype(F32)
            xb = xf[xs * NY + 2 * k + 1].astype(F32)
            ssq = ssq + xa * xa + xb * xb
            ta_i = 8 * k + xs
            tb_i = 8 * k + 4 + xs
            ga = gd2[xs % 2, pl.ds(4 * k + xs // 2, 1), :]
            gb = gd2[xs % 2, pl.ds(4 * k + 2 + xs // 2, 1), :]
            v = jnp.concatenate([xa * ga, xb * gb], axis=1)
            lhs = jnp.concatenate(
                [jnp.where(lo256, v, 0.0).astype(BF16), jnp.where(lo256, 0.0, v).astype(BF16)], axis=0
            )
            rhs = jnp.concatenate(
                [wi[ta_i].reshape(128, 256), wi[tb_i].reshape(128, 256)], axis=0
            )
            acc = acc + jnp.dot(lhs, rhs, preferred_element_type=F32)
        return acc, ssq

    acc = jnp.zeros((256, 256), F32)
    ssq = jnp.zeros((128, 128), F32)
    acc, ssq = slab(x, acc, ssq)
    for k in (1, 3, 5, 7):
        arrived(xf.at[xm * NY + at_y(NEAR[k])], rdl.at[k])
    acc, ssq = slab(xm, acc, ssq)
    for k in (0, 2, 4, 6):
        arrived(xf.at[xp * NY + at_y(NEAR[k])], rdr.at[k])
    acc, ssq = slab(xp, acc, ssq)
    for k in range(8):
        arrived(xf.at[xo * NY + at_y(NEAR[k])], rdo.at[k])
    acc, ssq = slab(xo, acc, ssq)

    s0 = jnp.sum(jnp.where(lo128, ssq, 0.0), axis=1, keepdims=True)
    s1 = jnp.sum(jnp.where(lo128, 0.0, ssq), axis=1, keepdims=True)
    scale = lax.rsqrt(jnp.concatenate([s0, s1], axis=0) / 2048.0 + EPS)
    gate, up = acc[:, 0:128] * scale, acc[:, 128:256] * scale
    hidden = (jax.nn.silu(gate) * up).astype(BF16)
    hid = jnp.concatenate([hidden[0:128], hidden[128:256]], axis=1)

    def share(xs, k):
        i = xs * NY + at_y(FAR[k])
        yf[i] = jnp.dot(hid, wd2[i], preferred_element_type=F32).astype(BF16)

    for k in range(8):
        share(xo, k)
        src = yf.at[xo * NY + at_y(FAR[k])]
        push(src, ro.at[k], se, reo.at[k], dx=xp if k % 2 == 0 else xm)
    for k in range(8):
        share(xp, k)
        share(xm, k)
        src_p, src_m = yf.at[xp * NY + at_y(FAR[k])], yf.at[xm * NY + at_y(FAR[k])]
        if k % 2 == 0:
            push(src_m, rr.at[k], se, rer.at[k], dx=xm)
        else:
            push(src_p, rl.at[k], se, rel.at[k], dx=xp)
    for k in range(8):
        i_p, i_m = xp * NY + at_y(FAR[k]), xm * NY + at_y(FAR[k])
        arrived(ro.at[k], reo.at[k])
        if k % 2 == 0:
            yf[i_p] = (yf[i_p].astype(F32) + ro[k].astype(F32)).astype(BF16)
            push(yf.at[i_p], rl.at[k], se, rel.at[k], dx=xp)
        else:
            yf[i_m] = (yf[i_m].astype(F32) + ro[k].astype(F32)).astype(BF16)
            push(yf.at[i_m], rr.at[k], se, rer.at[k], dx=xm)
    total = None
    for k in range(8):
        i = x * NY + at_y(FAR[k])
        own = jnp.dot(hid, wd2[i], preferred_element_type=F32)
        arrived(rl.at[k], rel.at[k])
        arrived(rr.at[k], rer.at[k])
        total = own + rl[k].astype(F32) + rr[k].astype(F32)
        if FAR[k] != 0:
            yf[i] = total.astype(BF16)
            push(yf.at[i], ry.at[FAR[k] - 1], se, rey.at[FAR[k] - 1], dy=FAR[k])
    for d in (1, 7, 2, 6, 3, 5, 4):
        arrived(ry.at[d - 1], rey.at[d - 1])
        total = total + ry[d - 1].astype(F32)

    ZPACK(qs, total)
    qr[e] = qs[e]
    to_ep(qs, qr, sq, rq)
    all_of(qr, sq, rq).wait_recv()
    back = ZUNPACK(qr).astype(F32)
    a0 = jnp.dot(wtv[0], back, precision=HI, preferred_element_type=F32)
    a1 = jnp.dot(wtv[1], back, precision=HI, preferred_element_type=F32)
    comb = jnp.where(lo64, a0, a1)
    out_ref[...] = (tokd[...] + (comb + swap(comb)))[:, 0:64].astype(BF16)

    all_of(ta, sa, ra).wait_send()
    all_of(wo, sw, rw_sem).wait_send()
    all_of(ma, sm, rm).wait_send()
    all_of(zs, sz, rz).wait_send()
    all_of(qs, sq, rq).wait_send()
    all_of(xf, sx, rz).wait_send()
    all_of(yf, se, rz).wait_send()


def ZPACK(ref, v):
    ref[...] = v.reshape(ZSHAPE).astype(BF16)


def ZUNPACK(ref):
    return ref[...].reshape(128, 128)


ZSHAPE = (32, 4, 128)


def local(
    tokens, mix_gain, w_in, a_real, a_imag, log_step, b_coef, output_coefficients, skip, w_out,
    state, ffn_gain, w_gate, w_up, w_down, expert_ids, route_weights,
):
    vm = pl.BlockSpec(memory_space=pltpu.VMEM)
    hbm = pl.BlockSpec(memory_space=pl.ANY)
    smem = pl.BlockSpec(memory_space=pltpu.SMEM)
    dma = pltpu.SemaphoreType.DMA
    V = pltpu.VMEM
    return pl.pallas_call(
        body,
        name="layer",
        out_shape=(
            jax.ShapeDtypeStruct(tokens.shape, BF16),
            jax.ShapeDtypeStruct(state.shape, F32),
        ),
        in_specs=[
            vm, vm, hbm, vm, vm, smem, vm, vm, vm, vm, vm, vm, hbm, hbm, hbm, vm, vm,
        ],
        out_specs=(vm, vm),
        scratch_shapes=[
            V((32, 32, 128), BF16),
            V((32, 16, 128), BF16),
            V((32, 16, 128), BF16),
            V((32, 16, 128), BF16),
            V(ZSHAPE, BF16),
            V(ZSHAPE, BF16),
            V((32, 128, 128), BF16),
            V((32, 128, 128), BF16),
            V((8, 128, 128), BF16),
            V((8, 128, 128), BF16),
            V((8, 128, 128), BF16),
            V((7, 128, 128), BF16),
            V(ZSHAPE, BF16),
            V(ZSHAPE, BF16),
            V((32, 2, 64, 32), BF16),
            V((32, 2, 64, 256), BF16),
            V((2, 128, 2048), BF16),
            V((32, 256, 128), BF16),
            V((2, 16, 128), F32),
            V((2, 16, 128), F32),
            V((128, 128), BF16),
            V((2, 64, 128), F32),
            V((64, 128), F32),
            dma((7,)),
            dma, dma, dma, dma, dma, dma, dma,
            dma, dma, dma, dma, dma,
            dma((8,)), dma((8,)), dma((8,)), dma((8,)),
            dma((8,)), dma((8,)), dma((8,)), dma((7,)),
        ],
        compiler_params=pltpu.CompilerParams(
            collective_id=0, has_side_effects=True, vmem_limit_bytes=48 * 1024 * 1024
        ),
    )(
        tokens, mix_gain.reshape(16, 128), w_in.reshape(32, 64, 32), a_real, a_imag, log_step,
        b_coef, output_coefficients, skip.reshape(1, 32), w_out, state, ffn_gain.reshape(16, 128),
        w_gate.reshape(2, 32, 64, 128), w_up.reshape(2, 32, 64, 128), w_down, expert_ids,
        route_weights,
    )


def solution(mesh):
    in_specs = (
        P("ep", "tp"), P(), P(None, "tp"), P("tp", None), P("tp", None), P("tp"),
        P(None, "tp", None, None), P(None, "tp", None, None), P("tp"), P("tp", None),
        P(None, "ep", "tp", None), P(), P("ep", None, "tp"), P("ep", None, "tp"),
        P("ep", "tp", None), P("ep", None), P("ep", None),
    )
    out_specs = (P("ep", "tp"), P(None, "ep", "tp", None))
    return jax.shard_map(local, mesh=mesh, in_specs=in_specs, out_specs=out_specs, check_vma=False)
```

time: 218 us -> 101 us (0.46)
  blocking collectives: 103 us -> 0 us
  Pallas kernels: 0 us -> 91.3 us
  waiting for transfers between devices: 39.2 us -> 0 us
  local copies, waits for them, and re-layouts: 38.4 us -> 8.35 us
  starting transfers between devices: 25.4 us -> 0 us
  matrix products: 5.27 us -> 0 us
  other arithmetic: 4.97 us -> 0 us
    all_to_all x3 -> x0, blocking collectives: 103 us -> none  [the longest x1 40.2 us: local(): lax.all_to_all(send_buffer, 'ep', split_axis=0, concat_axis=0, tiled=True)]
    pallas_call x0 -> x1, Pallas kernels: none -> 91.3 us  [local(): pl.pallas_call(body, name='layer', out_shape=(jax.ShapeDtypeStruct(tokens...]
    all_to_all x4 -> x0, waiting for transfers between devices: 39.2 us -> none  [the longest x2 15.7 us: sent_to_all(): lax.all_to_all(jnp.broadcast_to(x[None], (devices, *x.shape)), axis, 0, 0...]
    all_to_all x4 -> x0, starting transfers between devices: 25.4 us -> none  [the longest x2 14.3 us: sent_to_all(): lax.all_to_all(jnp.broadcast_to(x[None], (devices, *x.shape)), axis, 0, 0...]
    unnamed x37 -> x34, local copies, waits for them, and re-layouts: 19.5 us -> 8.35 us
    reshape x5 -> x0, local copies, waits for them, and re-layouts: 9.98 us -> none  [the longest x4 6.52 us: cut_along(): return jnp.moveaxis(x.reshape(*before, devices, -1, *after), dim, 0)]
    dot_general x10 -> x0, matrix products: 5.27 us -> none  [the longest x1 2.91 us: local(): jnp.einsum('njcf,jfd->njcd', hidden, w_down, preferred_element_type=jnp.f...]
    transpose x2 -> x0, local copies, waits for them, and re-layouts: 3.15 us -> none  [laid_out(): pieces = jnp.moveaxis(pieces, 0, dim)]
  transfers between devices with their start and end apart: 4 -> 0, of which waited for: 4 -> 0; matrix products, arithmetic and copies ran while one was open for 2% -> 0% of each run, Pallas kernels for 0% -> 0%
where the time goes in v1:
time: 101 us; the launch traced here: 100 us
  Pallas kernels  91.3 us (90%)
  local copies, waits for them, and re-layouts  8.35 us (8%)
    pallas_call x1, Pallas kernels, local(): pl.pallas_call(body, name='layer', out_shape=(jax.ShapeDtypeStruct(tokens...  91.3 us
    unnamed x34, local copies, waits for them, and re-layouts  8.35 us

profile of v1, /device:TPU:1, one launch (start us, length us, event | category | flops | bytes accessed | tf_op | source)
XLA Modules:
  0.0 100.4 jit_solution(218009747581278551)
XLA Ops:
  0.6 0.0 copy-start.13
  0.6 0.8 copy.21.ids_ref
  1.4 0.8 copy.22.rw_ref
  2.2 0.8 copy.20.b_ref
  3.1 0.0 copy-done.13
  3.1 0.0 copy-start.3
  3.1 0.0 copy-start.4
  3.1 0.0 copy-start.5
  3.1 0.0 copy-start.6
  3.1 0.0 copy-start.7
  3.1 0.0 copy-start.8
  3.1 0.0 copy-start.10
  3.2 0.0 copy-start.12
  3.2 0.3 copy.19
  3.5 0.0 copy-start.9
  3.5 0.0 copy-start.11
  3.5 0.5 copy-done.3
  4.0 0.1 copy-done.4
  4.0 0.0 copy-done.5
  4.0 0.0 copy-done.6
  4.1 0.0 copy-done.7
  4.1 0.0 copy-done.8
  4.1 0.0 copy-done.10
  4.1 0.0 copy-done.12
  4.1 0.1 copy-done.9
  4.2 0.0 copy-done.11
  4.2 1.2 %copy-done = bf16[2,2048,128]{2,1,0:T(8,128)(2,1)S(1)} copy-done((bf16[2,2048,128]{2,1,0:T(8,128)(2,1)S(1)}, bf16[2,2048,128]{2,1,0:T(8,128)(2,1)}, u32[]{:S(2)}) %copy-start) | copy-done | bytes 1048600
  5.4 1.2 %copy-done.1 = bf16[2,2048,128]{2,1,0:T(8,128)(2,1)S(1)} copy-done((bf16[2,2048,128]{2,1,0:T(8,128)(2,1)S(1)}, bf16[2,2048,128]{2,1,0:T(8,128)(2,1)}, u32[]{:S(2)}) %copy-start.1) | copy-done | bytes 1048600
  6.6 1.2 %copy-done.2 = bf16[2,128,2048]{2,1,0:T(8,128)(2,1)S(1)} copy-done((bf16[2,128,2048]{2,1,0:T(8,128)(2,1)S(1)}, bf16[2,128,2048]{2,1,0:T(8,128)(2,1)}, u32[]{:S(2)}) %copy-start.2) | copy-done | bytes 1048600
  7.9 91.3 %layer.1 = (bf16[64,64]{1,0:T(8,128)(2,1)S(1)}, f32[2,64,2,64]{3,2,1,0:T(2,128)S(1)}) custom-call(bf16[64,64]{1,0:T(8,128)(2,1)S(1)} %copy-done.6, f32[16,128]{1,0:T(8,128)S(1)} %bitcast.9, bf16[32,64,32]{2,1,0:T(8,128)(2,1)S(1)} %bitcast.6, f32[2,64]{1,0:T(2,128)S(1)} %copy-done.9, f32[2,64]{1,0:T(2,128)S(1)} %copy-done.10, f32[2]{0:T(128)S(1)} %copy-done.11, ...), custom_call_target="tpu_custom_call" | custom-call | tf_op jit(solution)/shard_map/layer/pallas_call | solution.py:416
  99.2 0.6 copy.25
  99.8 0.7 copy.26
  (3 shorter events, 0.0 us)
Async XLA Ops:
  0.6 2.4 %copy-start.13 = (bf16[2048,32]{0,1:T(8,128)(2,1)S(1)}, bf16[2048,32]{0,1:T(8,128)(2,1)}, u32[]{:S(2)}) copy-start(bf16[2048,32]{0,1:T(8,128)(2,1)} %param.19) | copy-start | bytes 393220
  3.1 0.9 copy-start.3
  3.1 1.0 copy-start.4
  3.1 1.0 copy-start.5
  3.1 0.9 copy-start.6
  3.1 0.9 copy-start.7
  3.1 0.9 copy-start.8
  3.1 0.9 copy-start.10
  3.2 0.9 copy-start.12
  3.5 0.7 copy-start.9
  3.5 0.7 copy-start.11
  4.2 1.2 %copy-start = (bf16[2,2048,128]{2,1,0:T(8,128)(2,1)S(1)}, bf16[2,2048,128]{2,1,0:T(8,128)(2,1)}, u32[]{:S(2)}) copy-start(bf16[2,2048,128]{2,1,0:T(8,128)(2,1)} %param.29) | copy-start | bytes 3145732
  5.4 1.2 %copy-start.1 = (bf16[2,2048,128]{2,1,0:T(8,128)(2,1)S(1)}, bf16[2,2048,128]{2,1,0:T(8,128)(2,1)}, u32[]{:S(2)}) copy-start(bf16[2,2048,128]{2,1,0:T(8,128)(2,1)} %param.30) | copy-start | bytes 3145732
  6.6 1.2 %copy-start.2 = (bf16[2,128,2048]{2,1,0:T(8,128)(2,1)S(1)}, bf16[2,128,2048]{2,1,0:T(8,128)(2,1)}, u32[]{:S(2)}) copy-start(bf16[2,128,2048]{2,1,0:T(8,128)(2,1)} %wd_hbm.1) | copy-start | bytes 3145732

commit v2 on v1

v2 whole, which is shorter than its diff:
```python
import jax
import jax.numpy as jnp
from jax import lax
from jax.experimental import pallas as pl
from jax.experimental.pallas import tpu as pltpu
from jax.sharding import PartitionSpec as P

EPS = 1e-06
HI = lax.Precision.HIGHEST
MESH = pl.DeviceIdType.MESH
NT = (((1,), (1,)), ((), ()))
TN = (((0,), (0,)), ((), ()))
F32 = jnp.float32
BF16 = jnp.bfloat16
NX, NY = 4, 8
TP, EP = 32, 32
NEAR = (0, 1, 7, 2, 6, 3, 5, 4)
FAR = (4, 3, 5, 2, 6, 1, 7, 0)


def iota(shape, dim):
    return lax.broadcasted_iota(jnp.int32, shape, dim)


def lo_lanes(rows, lanes=128):
    return iota((rows, lanes), 1) % 128 < 64


def swap(x):
    return pltpu.roll(x, 64, axis=x.ndim - 1)


def far_first(i):
    return 16 + ((i + 1) // 2) * (2 * (i % 2) - 1) * -1


def out_far(i):
    return 16 + ((i + 1) // 2) * (2 * (i % 2) - 1)


def out_near(i):
    return (1 - i % 2) * (8 - i // 2) - (i % 2) * (7 - i // 2)


def back_far(i):
    return 16 + ((i + 1) // 2) * (1 - 2 * (i % 2))


def back_near(i):
    return -out_near(i)


def body(
    tok_hbm, gain1_hbm, win_hbm, ar_hbm, ai_hbm, ls_hbm, b_hbm, oc_hbm, skip_hbm, wout_hbm,
    state_hbm, gain2_hbm, wg_hbm, wu_hbm, wd_hbm, ids_hbm, rw_hbm,
    out_hbm, ns_hbm, out_ref, ns_ref,
    tok_ref, gain1_ref, win_ref, ar_ref, ai_ref, ls_ref, b_ref, oc_ref, skip_ref, wout_ref,
    state_ref, gain2_ref, ids_ref, rw_ref,
    ta, ma, ws, wo, zs, zr, xf, yf, ro, rl, rr, ry, qs, qr, win2, wi, wdr, wd2,
    gd1, gd2, seltv, wtv, tokd,
    load_sem, put_sem, sa, sw, sv, sm, sz, sx, se, sq, ra, ray, rw_sem, rv, rm, rz, rq,
    rdy, rdl, rdr, rdo, reo, rel, rer, rey,
):
    t = lax.axis_index("tp")
    e = lax.axis_index("ep")
    y = t // NX
    x = t % NX
    xp = lax.rem(x + 1, NX)
    xm = lax.rem(x + NX - 1, NX)
    xo = lax.rem(x + 2, NX)

    loads = {}

    def load(name, src, dst):
        c = pltpu.make_async_copy(src, dst, load_sem.at[len(loads)])
        loads[name] = c
        c.start()

    load("tok", tok_hbm, tok_ref)
    load("wout", wout_hbm, wout_ref)
    barrier = pltpu.get_barrier_semaphore()

    def greet(i, c):
        d = far_first(i)
        pl.semaphore_signal(
            barrier, inc=1, device_id={"ep": lax.rem(e + d, EP)}, device_id_type=MESH
        )
        pl.semaphore_signal(
            barrier, inc=1, device_id={"tp": lax.rem(t + d, TP)}, device_id_type=MESH
        )
        return c

    lax.fori_loop(0, 31, greet, 0)
    load("ids", ids_hbm, ids_ref)
    load("rw", rw_hbm, rw_ref)
    load("gain1", gain1_hbm, gain1_ref)
    load("gain2", gain2_hbm, gain2_ref)
    load("win", win_hbm, win_ref)
    load("wd", wd_hbm, wdr)
    load("ar", ar_hbm, ar_ref)
    load("ai", ai_hbm, ai_ref)
    load("ls", ls_hbm, ls_ref)
    load("b", b_hbm, b_ref)
    load("oc", oc_hbm, oc_ref)
    load("skip", skip_hbm, skip_ref)
    load("state", state_hbm, state_ref)
    for j in range(2):
        load(f"g{j}", wg_hbm.at[j], wi.at[:, j, :, pl.ds(0, 128)])
        load(f"u{j}", wu_hbm.at[j], wi.at[:, j, :, pl.ds(128, 128)])
    loads["tok"].wait()

    tok = tok_ref[...]
    spread = (iota((64, 128), 1) % 64 == iota((64, 128), 0)).astype(F32)
    lo64 = lo_lanes(64)
    spread_lo = jnp.where(lo64, spread, 0.0).astype(BF16)
    spread_hi = jnp.where(lo64, 0.0, spread).astype(BF16)
    packed = jnp.dot(tok[0:32], spread_lo, preferred_element_type=F32) + jnp.dot(
        tok[32:64], spread_hi, preferred_element_type=F32
    )
    ta[t] = packed.astype(BF16)
    tokd[...] = jnp.dot(tok, spread.astype(BF16), preferred_element_type=F32)

    loads["wout"].wait()
    lo16 = lo_lanes(16)
    for k in range(16):
        blk = wout_ref[:, k * 128 : (k + 1) * 128].astype(F32)
        top, bot = blk[0:16], blk[16:32]
        ws[2 * k] = jnp.where(lo16, top, swap(bot)).astype(BF16)
        ws[2 * k + 1] = jnp.where(lo16, swap(top), bot).astype(BF16)
    @pl.when(y // 2 == lax.rem(e, 4))
    def _():
        wo[t] = ws[t]


    for name in ("ids", "rw", "gain1", "gain2", "win"):
        loads[name].wait()
    twice = spread.astype(BF16)
    ids = jnp.dot(
        ids_ref[...].astype(F32).astype(BF16), twice, preferred_element_type=F32
    ).astype(jnp.int32)
    rw = jnp.dot(rw_ref[...], spread, precision=HI, preferred_element_type=F32)
    slot = iota((128, 128), 0)
    named = 2 * (slot // 4) + iota((128, 128), 1) // 64
    hit0 = (ids[0:1] == named).astype(F32)
    hit1 = (ids[1:2] == named).astype(F32)
    hit = hit0 + hit1
    a_i, b_i = iota((128, 128), 0), iota((128, 128), 1)
    before = jnp.logical_and(a_i < b_i, a_i // 64 == b_i // 64).astype(F32).astype(BF16)
    rank = jnp.dot(hit.astype(BF16), before, preferred_element_type=F32)
    here = (rank.astype(jnp.int32) == slot % 4).astype(F32)
    seltv[...] = (hit * here).astype(BF16)
    wtv[...] = ((hit0 * rw[0:1] + hit1 * rw[1:2]) * here).T

    for src, dst in ((gain1_ref, gd1), (gain2_ref, gd2)):
        g = src[...]
        s = swap(g)
        lo = lo_lanes(16)
        dst[0] = jnp.where(lo, g, s)
        dst[1] = jnp.where(lo, s, g)

    lo32 = lo_lanes(32)
    for k in range(16):
        blk = win_ref[:, k * 128 : (k + 1) * 128].astype(F32)
        other = swap(blk)
        c = 256 * k
        win2[:, c : c + 128] = jnp.where(lo32, blk, other).astype(BF16)
        win2[:, c + 128 : c + 256] = jnp.where(lo32, other, blk).astype(BF16)
    loads["wd"].wait()
    lo128 = lo_lanes(128)
    for k in range(16):
        for j in range(2):
            blk = wdr[j, :, k * 128 : (k + 1) * 128].astype(F32)
            rolled = swap(blk)
            even, odd = (blk, rolled) if j == 0 else (rolled, blk)
            keep = lo128 if j == 0 else jnp.logical_not(lo128)
            for tt, piece in ((2 * k, even), (2 * k + 1, odd)):
                pos = (tt % NX) * NY + tt // NX
                wd2[pos, j * 128 : (j + 1) * 128, :] = jnp.where(keep, piece, 0.0).astype(BF16)
    pl.semaphore_wait(barrier, 62)

    def to_tp(src, dst, send, recv):
        def one(i, c):
            dest = lax.rem(t + far_first(i), TP)
            pltpu.make_async_remote_copy(
                src_ref=src(dest), dst_ref=dst, send_sem=send, recv_sem=recv,
                device_id={"tp": dest}, device_id_type=MESH,
            ).start()
            return c

        lax.fori_loop(0, 31, one, 0)

    def to_ep(ref_from, ref_to, count, shift, send, recv):
        def one(i, c):
            d = shift(i)
            dest = lax.rem(e + d + EP, EP)
            pltpu.make_async_remote_copy(
                src_ref=ref_from(dest, d), dst_ref=ref_to(d), send_sem=send, recv_sem=recv,
                device_id={"ep": dest}, device_id_type=MESH,
            ).start()
            return c

        lax.fori_loop(0, count, one, 0)

    def push(src, dst, ssem, rsem, dy=None, dx=None):
        py = y if dy is None else lax.rem(y + dy, NY)
        px = x if dx is None else dx
        pltpu.make_async_remote_copy(
            src_ref=src, dst_ref=dst, send_sem=ssem, recv_sem=rsem,
            device_id={"tp": py * NX + px}, device_id_type=MESH,
        ).start()

    def arrived(ref, rsem):
        pltpu.make_async_remote_copy(
            src_ref=ref, dst_ref=ref, send_sem=sx, recv_sem=rsem,
            device_id={"tp": lax.rem(t + 1, TP)}, device_id_type=MESH,
        ).wait_recv()

    def at_y(off):
        return lax.rem(y + off, NY)

    def offer(buf, ssem, ysem, xsem):
        ref = buf.at[t]
        for d in (4, 3, 5, 2, 6, 1, 7):
            push(ref, ref, ssem, ysem.at[d], dy=d)
        for px in (xo, xp, xm):
            push(ref, ref, ssem, xsem, dx=px)

    def pass_on(buf, ssem, ysem, xsem, between):
        for off in NEAR[1:]:
            ref = buf.at[at_y(off) * NX + x]
            arrived(ref, ysem.at[8 - off])
            for px in (xo, xp, xm):
                push(ref, ref, ssem, xsem, dx=px)
        between()
        arrived(buf.at[pl.ds(0, 24)], xsem)

    def all_of(ref, send, recv):
        r = ref.at[pl.ds(0, 31)]
        return pltpu.make_async_remote_copy(
            src_ref=r, dst_ref=r, send_sem=send, recv_sem=recv,
            device_id={"tp": lax.rem(t + 1, TP)}, device_id_type=MESH,
        )

    offer(ta, sa, ray, ra)
    row = lax.rem(e, 4)
    fetch = y // 2 == row

    @pl.when(fetch)
    def _():
        to_tp(lambda d: ws.at[d], wo.at[t], sw, rw_sem)


    for name in ("ar", "ai", "ls", "b", "oc", "skip", "state", "g0", "u0", "g1", "u1"):
        loads[name].wait()

    block = wo.at[pl.ds(row * 8, 8)]

    def share_projection():
        @pl.when(fetch)
        def _():
            arrived(wo.at[pl.ds(0, 7)], rw_sem)

        @pl.when(jnp.logical_not(fetch))
        def _():
            arrived(wo.at[pl.ds(0, 8)], rw_sem)

        for d in (2, 1, 3):
            pltpu.make_async_remote_copy(
                src_ref=block, dst_ref=block, send_sem=sv, recv_sem=rv,
                device_id={"ep": e - row + lax.rem(row + d, 4)}, device_id_type=MESH,
            ).start()

    pass_on(ta, sa, ray, ra, share_projection)
    acc = jnp.zeros((32, 128), F32)
    for k in range(TP):
        v = ta[k].astype(F32)
        acc = acc + v * v
    s0 = jnp.sum(jnp.where(lo32, acc, 0.0), axis=1, keepdims=True)
    s1 = jnp.sum(jnp.where(lo32, 0.0, acc), axis=1, keepdims=True)
    scale = jnp.where(
        lo32, lax.rsqrt(s0 / 2048.0 + EPS), lax.rsqrt(s1 / 2048.0 + EPS)
    )
    blocks = []
    for k in range(TP):
        v = ta[k].astype(F32) * scale * gd1[k % 2, k // 2 : k // 2 + 1, :]
        blocks.append(
            jnp.concatenate(
                [jnp.where(lo32, v, 0.0).astype(BF16), jnp.where(lo32, 0.0, v).astype(BF16)], axis=0
            )
        )
    drive = lax.dot_general(
        jnp.concatenate(blocks, axis=1), win2[...], NT, preferred_element_type=F32
    )
    drive = drive.astype(BF16).astype(F32)

    readout = skip_ref[...] * drive
    zeros16 = jnp.zeros((16, 64), F32)
    for g in range(2):
        step = jnp.exp(ls_ref[:, g : g + 1])
        ar, ai = ar_ref[g : g + 1, :], ai_ref[g : g + 1, :]
        mag = jnp.exp(step * ar)
        dr, di = mag * jnp.cos(step * ai), mag * jnp.sin(step * ai)
        den = ar * ar + ai * ai
        sh = dr - 1.0
        fr, fi = (sh * ar + di * ai) / den, (di * ar - sh * ai) / den
        u = drive[:, g * 16 : (g + 1) * 16]
        q0 = jnp.dot(u, b_ref[0, g], precision=HI, preferred_element_type=F32)
        q1 = jnp.dot(u, b_ref[1, g], precision=HI, preferred_element_type=F32)
        p0, p1 = state_ref[0, :, g, :], state_ref[1, :, g, :]
        n0 = dr * p0 - di * p1 + (fr * q0 - fi * q1)
        n1 = dr * p1 + di * p0 + (fr * q1 + fi * q0)
        ns_ref[0, :, g, :] = n0
        ns_ref[1, :, g, :] = n1
        order = (lambda o: [o, zeros16]) if g == 0 else (lambda o: [zeros16, o])
        c0 = jnp.concatenate(order(oc_ref[0, g]), axis=0)
        c1 = jnp.concatenate(order(oc_ref[1, g]), axis=0)
        readout = readout + (
            lax.dot_general(n0, c0, NT, precision=HI, preferred_element_type=F32)
            - lax.dot_general(n1, c1, NT, precision=HI, preferred_element_type=F32)
        )
    put_state = pltpu.make_async_copy(ns_ref, ns_hbm, put_sem.at[0])
    put_state.start()
    mixed = jax.nn.gelu(readout)
    first = iota((64, 32), 1) < 16
    stacked = jnp.concatenate(
        [jnp.where(first, mixed, 0.0), jnp.where(first, 0.0, mixed)], axis=0
    ).astype(BF16)
    pick = (iota((16, 32), 1) % 16 == iota((16, 32), 0)).astype(F32).astype(BF16)
    ma[t] = lax.dot_general(pick, stacked, NT, preferred_element_type=F32).astype(BF16)
    to_tp(lambda d: ma.at[t], ma.at[t], sm, rm)
    all_of(ma, sm, rm).wait_recv()
    arrived(wo.at[pl.ds(0, 24)], rv)
    prod = lax.dot_general(
        ma[...].reshape(512, 128), wo[...].reshape(512, 128), TN, preferred_element_type=F32
    )
    half = jnp.where(lo64, prod[0:64], prod[64:128])
    resid = (tokd[...] + (half + swap(half))).astype(BF16)
    resid_f = resid.astype(F32)
    tokd[...] = resid_f

    zero = jnp.zeros((64, 128), F32)
    diag = jnp.concatenate(
        [jnp.where(lo64, resid_f, zero), jnp.where(lo64, zero, resid_f)], axis=0
    ).astype(BF16)
    sent = jnp.dot(seltv[...], diag, preferred_element_type=F32)
    ZPACK(zs, sent)
    zr[8] = zs[e]
    for c, count, shift in ((1, 16, out_far), (0, 15, out_near)):
        to_ep(
            lambda dest, d: zs.at[dest], lambda d: zr.at[lax.rem(40 - d, EP)], count, shift, sz,
            rz.at[c],
        )

    def part(c, i):
        return xf.at[i, pl.ds(64 * c, 64)]

    def begin(c):
        arrived(zr.at[pl.ds(0, 15 + c)], rz.at[c])
        xf[x * NY + y, 64 * c : 64 * c + 64, :] = zr[16 * c : 16 * c + 16].reshape(64, 128)
        ref = part(c, x * NY + y)
        for d in (1, 7, 2, 6):
            push(ref, ref, sx, rdy.at[c, d], dy=d)
        push(ref, ref, sx, rdl.at[c, 0], dx=xp)
        push(ref, ref, sx, rdr.at[c, 0], dx=xm)

    def onward(c, k):
        ref = part(c, x * NY + at_y(NEAR[k]))
        arrived(ref, rdy.at[c, 8 - NEAR[k]])
        if NEAR[k] == 2:
            push(ref, ref, sx, rdy.at[c, 5], dy=7)
            if c == 0:
                push(ref, ref, sx, rdy.at[c, 4], dy=6)
        if NEAR[k] == 6:
            push(ref, ref, sx, rdy.at[c, 3], dy=1)
            if c == 1:
                push(ref, ref, sx, rdy.at[c, 4], dy=2)
        push(ref, ref, sx, rdl.at[c, k], dx=xp)
        push(ref, ref, sx, rdr.at[c, k], dx=xm)

    def relay(c, k):
        yk = at_y(NEAR[k])
        if k % 2 == 0:
            ref = part(c, xm * NY + yk)
            arrived(ref, rdl.at[c, k])
            push(ref, ref, sx, rdo.at[c, k], dx=xp)
        else:
            ref = part(c, xp * NY + yk)
            arrived(ref, rdr.at[c, k])
            push(ref, ref, sx, rdo.at[c, k], dx=xm)

    begin(0)
    for k in range(1, 5):
        onward(0, k)
    begin(1)
    for k in range(5, 8):
        onward(0, k)
        relay(0, k - 5)
    for k in range(1, 5):
        onward(1, k)
        relay(0, k + 2)
    relay(0, 7)
    for k in range(5, 8):
        onward(1, k)
        relay(1, k - 5)
    for k in range(3, 8):
        relay(1, k)

    lo256 = lo_lanes(128, 256)

    def slab(xs, acc, ssq):
        for k in range(4):
            xa = xf[xs * NY + 2 * k].astype(F32)
            xb = xf[xs * NY + 2 * k + 1].astype(F32)
            ssq = ssq + xa * xa + xb * xb
            ta_i = 8 * k + xs
            tb_i = 8 * k + 4 + xs
            ga = gd2[xs % 2, pl.ds(4 * k + xs // 2, 1), :]
            gb = gd2[xs % 2, pl.ds(4 * k + 2 + xs // 2, 1), :]
            v = jnp.concatenate([xa * ga, xb * gb], axis=1)
            lhs = jnp.concatenate(
                [jnp.where(lo256, v, 0.0).astype(BF16), jnp.where(lo256, 0.0, v).astype(BF16)], axis=0
            )
            rhs = jnp.concatenate(
                [wi[ta_i].reshape(128, 256), wi[tb_i].reshape(128, 256)], axis=0
            )
            acc = acc + jnp.dot(lhs, rhs, preferred_element_type=F32)
        return acc, ssq

    acc = jnp.zeros((256, 256), F32)
    ssq = jnp.zeros((128, 128), F32)
    acc, ssq = slab(x, acc, ssq)
    for c in range(2):
        for k in (1, 3, 5, 7):
            arrived(part(c, xm * NY + at_y(NEAR[k])), rdl.at[c, k])
    acc, ssq = slab(xm, acc, ssq)
    for c in range(2):
        for k in (0, 2, 4, 6):
            arrived(part(c, xp * NY + at_y(NEAR[k])), rdr.at[c, k])
    acc, ssq = slab(xp, acc, ssq)
    for c in range(2):
        for k in range(8):
            arrived(part(c, xo * NY + at_y(NEAR[k])), rdo.at[c, k])
    acc, ssq = slab(xo, acc, ssq)

    s0 = jnp.sum(jnp.where(lo128, ssq, 0.0), axis=1, keepdims=True)
    s1 = jnp.sum(jnp.where(lo128, 0.0, ssq), axis=1, keepdims=True)
    scale = lax.rsqrt(jnp.concatenate([s0, s1], axis=0) / 2048.0 + EPS)
    gate, up = acc[:, 0:128] * scale, acc[:, 128:256] * scale
    hidden = (jax.nn.silu(gate) * up).astype(BF16)
    hid = jnp.concatenate([hidden[0:128], hidden[128:256]], axis=1)

    def share(xs, k):
        i = xs * NY + at_y(FAR[k])
        yf[i] = jnp.dot(hid, wd2[i], preferred_element_type=F32).astype(BF16)

    def rows(ref, c, i):
        return ref.at[i, pl.ds(64 * c, 64)]

    def to_far(c, k):
        src = rows(yf, c, xo * NY + at_y(FAR[k]))
        push(src, rows(ro, c, k), se, reo.at[c, k], dx=xp if k % 2 == 0 else xm)

    def to_next(c, k):
        if k % 2 == 0:
            push(rows(yf, c, xm * NY + at_y(FAR[k])), rows(rr, c, k), se, rer.at[c, k], dx=xm)
        else:
            push(rows(yf, c, xp * NY + at_y(FAR[k])), rows(rl, c, k), se, rel.at[c, k], dx=xp)

    def add_on(c, k):
        r = slice(64 * c, 64 * c + 64)
        arrived(rows(ro, c, k), reo.at[c, k])
        px = xp if k % 2 == 0 else xm
        i = px * NY + at_y(FAR[k])
        yf[i, r, :] = (yf[i, r, :].astype(F32) + ro[k, r, :].astype(F32)).astype(BF16)
        if k % 2 == 0:
            push(rows(yf, c, i), rows(rl, c, k), se, rel.at[c, k], dx=xp)
        else:
            push(rows(yf, c, i), rows(rr, c, k), se, rer.at[c, k], dx=xm)

    def over_y(c):
        r = slice(64 * c, 64 * c + 64)
        for k in range(8):
            i = x * NY + at_y(FAR[k])
            arrived(rows(rl, c, k), rel.at[c, k])
            arrived(rows(rr, c, k), rer.at[c, k])
            total = yf[i, r, :].astype(F32) + rl[k, r, :].astype(F32) + rr[k, r, :].astype(F32)
            if FAR[k] != 0:
                yf[i, r, :] = total.astype(BF16)
                dst = rows(ry, c, FAR[k] - 1)
                push(rows(yf, c, i), dst, se, rey.at[c, FAR[k]], dy=FAR[k])
        return total

    def finish(c, total):
        r = slice(64 * c, 64 * c + 64)
        for d in (1, 7, 2, 6, 3, 5, 4):
            arrived(rows(ry, c, d - 1), rey.at[c, d])
            total = total + ry[d - 1, r, :].astype(F32)
        qs[16 * c : 16 * c + 16] = total.reshape(16, 4, 128).astype(BF16)
        count, shift = (15, back_near) if c == 0 else (16, back_far)
        to_ep(lambda dest, d: qs.at[d + 8], lambda d: qr.at[e], count, shift, sq, rq)

    for k in range(8):
        share(xo, k)
        to_far(1, k)
    for k in range(8):
        share(xp, k)
        share(xm, k)
        to_next(1, k)
    for k in range(8):
        to_far(0, k)
    for k in range(8):
        add_on(1, k)
    for k in range(8):
        to_next(0, k)
    for k in range(8):
        share(x, k)
    for k in range(8):
        add_on(0, k)
    total = over_y(1)
    near_total = over_y(0)
    finish(1, total)
    finish(0, near_total)

    qr[e] = qs[8]
    all_of(qr, sq, rq).wait_recv()
    back = ZUNPACK(qr).astype(F32)
    both = jnp.dot(wtv[...], back, precision=HI, preferred_element_type=F32)
    comb = jnp.where(lo64, both[0:64], both[64:128])
    out_ref[...] = (tokd[...] + (comb + swap(comb)))[:, 0:64].astype(BF16)
    put_out = pltpu.make_async_copy(out_ref, out_hbm, put_sem.at[1])
    put_out.start()

    all_of(ta, sa, ra).wait_send()

    @pl.when(fetch)
    def _():
        all_of(wo, sw, rw_sem).wait_send()

    blocks = wo.at[pl.ds(0, 24)]
    pltpu.make_async_remote_copy(
        src_ref=blocks, dst_ref=blocks, send_sem=sv, recv_sem=rv,
        device_id={"tp": lax.rem(t + 1, TP)}, device_id_type=MESH,
    ).wait_send()
    all_of(ma, sm, rm).wait_send()
    all_of(zs, sz, rq).wait_send()
    all_of(qs, sq, rq).wait_send()
    all_of(xf, sx, rq).wait_send()
    all_of(yf, se, rq).wait_send()
    put_state.wait()
    put_out.wait()


def ZPACK(ref, v):
    ref[...] = v.reshape(ZSHAPE).astype(BF16)


def ZUNPACK(ref):
    return ref[...].reshape(128, 128)


ZSHAPE = (32, 4, 128)


def local(
    tokens, mix_gain, w_in, a_real, a_imag, log_step, b_coef, output_coefficients, skip, w_out,
    state, ffn_gain, w_gate, w_up, w_down, expert_ids, route_weights,
):
    hbm = pl.BlockSpec(memory_space=pltpu.HBM)
    dma = pltpu.SemaphoreType.DMA
    V = pltpu.VMEM
    return pl.pallas_call(
        body,
        name="layer",
        out_shape=(
            jax.ShapeDtypeStruct(tokens.shape, BF16),
            jax.ShapeDtypeStruct(state.shape, F32),
        ),
        in_specs=[hbm] * 17,
        out_specs=(hbm, hbm),
        scratch_shapes=[
            V((64, 64), BF16),
            V((2, 64, 2, 64), F32),
            V((64, 64), BF16),
            V((16, 128), F32),
            V((32, 2048), BF16),
            V((2, 64), F32),
            V((2, 64), F32),
            V((1, 2), F32),
            V((2, 2, 16, 64), F32),
            V((2, 2, 16, 64), F32),
            V((1, 32), F32),
            V((32, 2048), BF16),
            V((2, 64, 2, 64), F32),
            V((16, 128), F32),
            V((2, 64), jnp.int32),
            V((2, 64), F32),
            V((32, 32, 128), BF16),
            V((32, 16, 128), BF16),
            V((32, 16, 128), BF16),
            V((32, 16, 128), BF16),
            V(ZSHAPE, BF16),
            V(ZSHAPE, BF16),
            V((32, 128, 128), BF16),
            V((32, 128, 128), BF16),
            V((8, 128, 128), BF16),
            V((8, 128, 128), BF16),
            V((8, 128, 128), BF16),
            V((7, 128, 128), BF16),
            V(ZSHAPE, BF16),
            V(ZSHAPE, BF16),
            V((32, 4096), BF16),
            V((32, 2, 64, 256), BF16),
            V((2, 128, 2048), BF16),
            V((32, 256, 128), BF16),
            V((2, 16, 128), F32),
            V((2, 16, 128), F32),
            V((128, 128), BF16),
            V((128, 128), F32),
            V((64, 128), F32),
            dma((19,)),
            dma((2,)),
            dma, dma, dma, dma, dma, dma, dma, dma,
            dma, dma((8,)), dma, dma, dma,
            dma((2,)), dma,
            dma((2, 8)), dma((2, 8)), dma((2, 8)), dma((2, 8)),
            dma((2, 8)), dma((2, 8)), dma((2, 8)), dma((2, 8)),
        ],
        compiler_params=pltpu.CompilerParams(
            collective_id=0, has_side_effects=True, vmem_limit_bytes=67043328
        ),
    )(
        tokens, mix_gain.reshape(16, 128), w_in.T, a_real, a_imag,
        log_step.reshape(1, 2), b_coef.transpose(0, 1, 3, 2), output_coefficients, skip.reshape(1, 32), w_out, state, ffn_gain.reshape(16, 128),
        w_gate.reshape(2, 32, 64, 128), w_up.reshape(2, 32, 64, 128), w_down, expert_ids.T,
        route_weights.T,
    )


def solution(mesh):
    in_specs = (
        P("ep", "tp"), P(), P(None, "tp"), P("tp", None), P("tp", None), P("tp"),
        P(None, "tp", None, None), P(None, "tp", None, None), P("tp"), P("tp", None),
        P(None, "ep", "tp", None), P(), P("ep", None, "tp"), P("ep", None, "tp"),
        P("ep", "tp", None), P("ep", None), P("ep", None),
    )
    out_specs = (P("ep", "tp"), P(None, "ep", "tp", None))
    return jax.shard_map(local, mesh=mesh, in_specs=in_specs, out_specs=out_specs, check_vma=False)
```

time: 101 us -> 91.5 us (0.906)
  local copies, waits for them, and re-layouts: 8.35 us -> 2.89 us
  Pallas kernels: 91.3 us -> 87.8 us
    unnamed x34 -> x2, local copies, waits for them, and re-layouts: 8.35 us -> 2.89 us
    pallas_call x1, Pallas kernels: 91.3 us -> 87.8 us  [local(): pl.pallas_call(body, name='layer', out_shape=(jax.ShapeDtypeStruct(tokens...]
where the time goes in v2:
time: 91.5 us; the launch traced here: 91.3 us
  Pallas kernels  87.8 us (96%)
  local copies, waits for them, and re-layouts  2.89 us (3%)
    pallas_call x1, Pallas kernels, local(): pl.pallas_call(body, name='layer', out_shape=(jax.ShapeDtypeStruct(tokens...  87.8 us
    unnamed x2, local copies, waits for them, and re-layouts  2.89 us

profile of v2, /device:TPU:1, one launch (start us, length us, event | category | flops | bytes accessed | tf_op | source)
XLA Modules:
  0.0 91.3 jit_solution(4016978637647424546)
XLA Ops:
  0.6 87.8 %layer.1 = (bf16[64,64]{1,0:T(8,128)(2,1)}, f32[2,64,2,64]{3,2,1,0:T(2,128)}) custom-call(bf16[64,64]{1,0:T(8,128)(2,1)} %tok_hbm.1, f32[16,128]{1,0:T(8,128)} %bitcast.14, bf16[32,2048]{1,0:T(8,128)(2,1)} %bitcast.12, f32[2,64]{1,0:T(2,128)} %ar_hbm.1, f32[2,64]{1,0:T(2,128)} %ai_hbm.1, f32[1,2]{1,0:T(1,128)} %bitcast.18, f32[2,2,16,64]{3,2,1,0:T(8,128)} %bitcast.13, ...), custom_call_target="tpu_custom_call" | custom-call | tf_op jit(solution)/shard_map/layer/pallas_call | solution.py:571
  88.4 1.3 %copy.21 = bf16[64,64]{1,0:T(8,128)(2,1)} copy(bf16[64,64]{1,0:T(8,128)(2,1)} %get-tuple-element.4) | data formatting | bytes 16384
  89.7 1.6 %copy.22 = f32[2,64,2,64]{3,2,1,0:T(2,128)} copy(f32[2,64,2,64]{3,2,1,0:T(2,128)} %get-tuple-element.5) | data formatting | bytes 131072

commit v3 on v2

--- a/solution.py
+++ b/solution.py
@@ -358,7 +358,7 @@
         arrived(zr.at[pl.ds(0, 15 + c)], rz.at[c])
         xf[x * NY + y, 64 * c : 64 * c + 64, :] = zr[16 * c : 16 * c + 16].reshape(64, 128)
         ref = part(c, x * NY + y)
-        for d in (1, 7, 2, 6):
+        for d in (1, 7, 4, 3, 5, 2, 6):
             push(ref, ref, sx, rdy.at[c, d], dy=d)
         push(ref, ref, sx, rdl.at[c, 0], dx=xp)
         push(ref, ref, sx, rdr.at[c, 0], dx=xm)
@@ -366,14 +366,6 @@
     def onward(c, k):
         ref = part(c, x * NY + at_y(NEAR[k]))
         arrived(ref, rdy.at[c, 8 - NEAR[k]])
-        if NEAR[k] == 2:
-            push(ref, ref, sx, rdy.at[c, 5], dy=7)
-            if c == 0:
-                push(ref, ref, sx, rdy.at[c, 4], dy=6)
-        if NEAR[k] == 6:
-            push(ref, ref, sx, rdy.at[c, 3], dy=1)
-            if c == 1:
-                push(ref, ref, sx, rdy.at[c, 4], dy=2)
         push(ref, ref, sx, rdl.at[c, k], dx=xp)
         push(ref, ref, sx, rdr.at[c, k], dx=xm)
 

time: 91.5 us -> 91.5 us (level)
  no operation moved by 1% of the time
where the time goes in v3:
time: 91.5 us; the launch traced here: 91.3 us
  Pallas kernels  87.7 us (96%)
  local copies, waits for them, and re-layouts  2.89 us (3%)
    pallas_call x1, Pallas kernels, local(): pl.pallas_call(body, name='layer', out_shape=(jax.ShapeDtypeStruct(tokens...  87.7 us
    unnamed x2, local copies, waits for them, and re-layouts  2.89 us

profile of v3, /device:TPU:1, one launch (start us, length us, event | category | flops | bytes accessed | tf_op | source)
XLA Modules:
  0.0 91.3 jit_solution(7903741613506032117)
XLA Ops:
  0.6 87.7 %layer.1 = (bf16[64,64]{1,0:T(8,128)(2,1)}, f32[2,64,2,64]{3,2,1,0:T(2,128)}) custom-call(bf16[64,64]{1,0:T(8,128)(2,1)} %tok_hbm.1, f32[16,128]{1,0:T(8,128)} %bitcast.14, bf16[32,2048]{1,0:T(8,128)(2,1)} %bitcast.12, f32[2,64]{1,0:T(2,128)} %ar_hbm.1, f32[2,64]{1,0:T(2,128)} %ai_hbm.1, f32[1,2]{1,0:T(1,128)} %bitcast.18, f32[2,2,16,64]{3,2,1,0:T(8,128)} %bitcast.13, ...), custom_call_target="tpu_custom_call" | custom-call | tf_op jit(solution)/shard_map/layer/pallas_call | solution.py:563
  88.4 1.3 %copy.21 = bf16[64,64]{1,0:T(8,128)(2,1)} copy(bf16[64,64]{1,0:T(8,128)(2,1)} %get-tuple-element.4) | data formatting | bytes 16384
  89.7 1.6 %copy.22 = f32[2,64,2,64]{3,2,1,0:T(2,128)} copy(f32[2,64,2,64]{3,2,1,0:T(2,128)} %get-tuple-element.5) | data formatting | bytes 131072
